TPU v7x, 32 devices: a whole 2x2x4 slice. The times are simulated.
32 devices in a mesh: ep: 8 (over z, x), tp: 4 (over y, core).
Axes of the slice: x: 2, y: 2, z: 4, core: 2. Of those that a mesh axis runs over, the one named last changes fastest.
Arguments:
- stream: bfloat16 [2048, 3072], P('ep'), may hold values from -30 to 30
- ffn_gain: bfloat16 [3072], replicated, may hold values from 0.099609375 to 1.8984375
- chosen: int32 [8, 256], replicated, may hold values from 0 to 2047, as said below
- affinity: float32 [8, 256], P('ep'), may hold values from 0.5 to 2
- w_gate: bfloat16 [8, 3072, 3072], P('ep', None, 'tp'), may hold values from -0.109375 to 0.109375
- w_up: bfloat16 [8, 3072, 3072], P('ep', None, 'tp'), may hold values from -0.109375 to 0.109375
- w_down: bfloat16 [8, 3072, 3072], P('ep', 'tp'), may hold values from -0.109375 to 0.109375
- final_gain: bfloat16 [3072], P('tp'), may hold values from 0.099609375 to 1.8984375
Outputs:
- normed: bfloat16 [2048, 3072], P('ep', 'tp')
Inputs may be any that keep to these rules, and one draw needn't show every extreme that they name: `chosen`: row e holds 256 distinct token numbers in ascending order. Of the 256 tokens of one index of ep, each expert reads at least one and at most 48; in every draw some expert reads exactly 48 from some index.
All inputs are finite; a program needn't handle non-finite values.
Results may differ from a plain program's by a relative error of at most 0.015.
Values may be sent and summed in bfloat16 or wider, within the bound.
A program may use at most 128 MiB of HBM per device.

v0:
```python
import jax
import jax.numpy as jnp
from jax import lax
from jax.sharding import PartitionSpec as P

EPSILON = 1e-06


def on_device(stream, ffn_gain, chosen, affinity, w_gate, w_up, w_down, final_gain):
    tok_rows = stream.shape[0]
    model_width = stream.shape[1]
    experts = chosen.shape[0]
    picks = chosen.shape[1]
    ep_count = lax.axis_size("ep")
    tp_count = lax.axis_size("tp")
    device = lax.axis_index("ep")
    column = lax.axis_index("tp")
    share_width = model_width // tp_count
    slots = 3 * tok_rows // 16
    widened = stream.astype(jnp.float32)
    scale_in = lax.rsqrt(jnp.mean(widened * widened, axis=-1, keepdims=True) + EPSILON)
    normed_in = (widened * scale_in * ffn_gain.astype(jnp.float32)).astype(jnp.bfloat16)
    source = chosen // tok_rows
    counts = jnp.sum(
        (source[:, :, None] == jnp.arange(ep_count)[None, None, :]).astype(jnp.int32), axis=1
    )
    starts = jnp.cumsum(counts, axis=1) - counts
    slot_range = jnp.arange(slots, dtype=jnp.int32)
    own_start = jnp.take(starts, device, axis=1)
    own_count = jnp.take(counts, device, axis=1)
    send_pos = jnp.clip(own_start[:, None] + slot_range[None, :], 0, picks - 1)
    send_valid = slot_range[None, :] < own_count[:, None]
    local_tok = jnp.where(
        send_valid, jnp.take_along_axis(chosen, send_pos, axis=1) - device * tok_rows, 0
    )
    local_flat = local_tok.reshape(-1)
    row_source = jnp.take(source, device, axis=0)
    row_starts = jnp.take(starts, device, axis=0)
    arrival = (
        row_source * slots + jnp.arange(picks, dtype=jnp.int32) - jnp.take(row_starts, row_source)
    )
    gate_rows = w_gate[0]
    up_rows = w_up[0]
    own_columns = lax.dynamic_slice_in_dim(normed_in, column * share_width, share_width, 1)
    outgoing = jnp.take(own_columns, local_flat, axis=0).reshape(experts, slots, share_width)
    arrived = lax.all_to_all(outgoing, "ep", split_axis=0, concat_axis=0, tiled=True)
    shared = jnp.take(arrived.reshape(-1, share_width), arrival, axis=0)
    piece = lax.all_gather(shared, "tp", axis=1, tiled=True)
    gate = jnp.dot(piece, gate_rows, preferred_element_type=jnp.float32)
    up = jnp.dot(piece, up_rows, preferred_element_type=jnp.float32)
    hidden = (jax.nn.silu(gate) * up).astype(jnp.bfloat16)
    down_rows = w_down[0]
    piece = down_rows
    expert_cols = lax.psum_scatter(
        lax.dot_general(
            piece, hidden, (((0,), (1,)), ((), ())), preferred_element_type=jnp.float32
        ).astype(jnp.bfloat16),
        "tp",
        scatter_dimension=0,
        tiled=True,
    ).astype(jnp.float32)
    weighted = (expert_cols * affinity[0][None, :]).astype(jnp.bfloat16)
    slot_pos = jnp.clip(row_starts[:, None] + slot_range[None, :], 0, picks - 1)
    leaving = jnp.take(weighted, slot_pos.reshape(-1), axis=1).reshape(share_width, ep_count, slots)
    returned = lax.all_to_all(leaving, "ep", split_axis=1, concat_axis=1, tiled=True)
    placing = (
        (local_flat[:, None] == jnp.arange(tok_rows, dtype=jnp.int32)[None, :])
        & send_valid.reshape(-1)[:, None]
    ).astype(jnp.bfloat16)
    update = lax.dot_general(
        placing,
        returned.reshape(share_width, -1),
        (((0,), (1,)), ((), ())),
        preferred_element_type=jnp.float32,
    )
    own_stream = lax.dynamic_slice_in_dim(widened, column * share_width, share_width, 1)
    merged = own_stream + update
    totals = lax.psum(jnp.sum(merged * merged, axis=1), "tp")
    scale_out = lax.rsqrt(totals[:, None] / model_width + EPSILON)
    return (merged * scale_out * final_gain.astype(jnp.float32)[None, :]).astype(jnp.bfloat16)


def solution(mesh):
    return jax.shard_map(
        on_device,
        mesh=mesh,
        in_specs=(
            P("ep", None),
            P(),
            P(),
            P("ep", None),
            P("ep", None, "tp"),
            P("ep", None, "tp"),
            P("ep", "tp", None),
            P("tp"),
        ),
        out_specs=P("ep", "tp"),
        check_vma=False,
    )
```

profile of v0, /device:TPU:0, one launch (start us, length us, event | category | flops | bytes accessed | tf_op | source)
XLA Modules:
  0.0 147.9 jit_solution(17516107885632444721)
XLA Ops:
  6.5 1.8 %multiply_reduce_fusion = f32[256]{0:T(256)S(1)} fusion(bf16[256,3072]{1,0:T(8,128)(2,1)} %param.10), kind=kLoop, calls=%fused_computation.12 | loop fusion | flops 2359040 | bytes 1573888 | tf_op jit(solution)/shard_map/reduce_sum | solution.py:21
  8.3 1.8 %convert_element_type.34 = f32[256,3072]{1,0:T(8,128)S(1)} convert(bf16[256,3072]{1,0:T(8,128)(2,1)} %param.10) | non-fusion elementwise | flops 786432 | bytes 4718592 | tf_op jit(solution)/shard_map/convert_element_type | solution.py:20
  10.2 0.6 add_rsqrt_fusion.1
  11.2 0.2 select_reduce_fusion
  11.4 0.4 copy-done.2
  12.1 2.7 %gather_fusion.3 = s32[384]{0:T(512)S(1)} fusion(s32[8,256]{1,0:T(8,128)S(1)} %copy-done, s32[384]{0:T(512)S(1)} %reshape.493), kind=kCustom, calls=%fused_computation.3 | custom fusion | bytes 6144 | tf_op jit(solution)/shard_map/jit(take_along_axis)/gather | solution.py:34
  14.9 0.6 compare_and_fusion
  15.7 0.6 pad_clamp_fusion.2
  16.4 0.8 multiply_convert_fusion.2
  17.1 2.8 %gather_fusion = bf16[384,768]{1,0:T(8,128)(2,1)} fusion(bf16[256,768]{1,0:T(8,128)(2,1)S(1)} %multiply_convert_fusion.2, s32[1024]{0:T(1024)} %pad_clamp_fusion.2), kind=kCustom, calls=%fused_computation | custom fusion | bytes 1181184 | tf_op jit(solution)/shard_map/jit(_take)/gather | solution.py:45
  19.9 2.0 %broadcast_select_fusion = bf16[8,48,768]{2,1,0:T(8,128)(2,1)} fusion(bf16[8,48,768]{2,1,0:T(8,128)(2,1)} %bitcast.71, pred[8,48]{1,0:T(8,128)(4,1)} %get-tuple-element.51), kind=kLoop, calls=%fused_computation.20 | loop fusion | flops 294912 | bytes 1180032 | tf_op jit(solution)/shard_map/jit(_take)/select_n | solution.py:45
  21.9 7.3 %all-to-all-start = ((bf16[8,48,768]{2,1,0:T(8,128)(2,1)}), bf16[8,48,768]{2,1,0:T(8,128)(2,1)S(1)}, u32[]{:S(2)}, u32[]{:S(2)}) async-start(bf16[8,48,768]{2,1,0:T(8,128)(2,1)} %broadcast_select_fusion), calls=%async_computation | async-start | bytes 1179648 | tf_op jit(solution)/shard_map/all_to_all | solution.py:46
  29.2 0.7 broadcast_select_fusion.4
  29.9 0.7 fusion.39
  30.6 4.4 %compare_select_fusion.10 = (s32[256,1]{0,1:T(1,128)S(1)}, s32[1,256]{1,0:T(1,128)S(1)}) fusion(s32[]{:T(128)} %bitcast.4, s32[]{:T(128)} %bitcast.5, s32[]{:T(128)} %bitcast.6, s32[]{:T(128)} %bitcast.7, s32[]{:T(128)} %bitcast.8, s32[]{:T(128)} %bitcast.10, s32[]{:T(128)} %bitcast.9, s32[8,256]{1,0:T(8,128)S(1)} %add_select_fusion, s32[]{:T(128)S(6)} %select_n.268, ...), kind=kLoop, calls=%fused_computation.62 | loop fusion | flops 4096 | bytes 3105 | tf_op jit(solution)/shard_map/jit(_take)/gather | solution.py:40
  35.0 0.7 compare_and_fusion.2
  35.7 9.4 %all-to-all-done = bf16[8,48,768]{2,1,0:T(8,128)(2,1)S(1)} async-done(((bf16[8,48,768]{2,1,0:T(8,128)(2,1)}), bf16[8,48,768]{2,1,0:T(8,128)(2,1)S(1)}, u32[]{:S(2)}, u32[]{:S(2)}) %all-to-all-start) | async-done | bytes 589856 | tf_op jit(solution)/shard_map/all_to_all | solution.py:46
  45.1 1.2 gather_fusion.1
  46.3 0.9 broadcast_select_fusion.2
  47.2 18.8 %all-gather.2.cloned.1.call-done = bf16[256,3072]{1,0:T(8,128)(2,1)} async-done(((bf16[256,768]{1,0:T(8,128)(2,1)}), bf16[256,3072]{1,0:T(8,128)(2,1)}) %all-gather.2.cloned.1.call-update) | async-done | bytes 1572880 | tf_op jit(solution)/shard_map/all_gather | solution.py:48
  66.0 4.3 %fusion.4 = f32[256,768]{1,0:T(8,128)S(1)} fusion(bf16[256,3072]{1,0:T(8,128)(2,1)} %all-gather.2.cloned.1.call-done, bf16[1,3072,768]{2,1,0:T(8,128)(2,1)} %param.14), kind=kOutput, calls=%fused_computation.8 | convolution fusion | flops 1207959552 | bytes 7077888 | tf_op jit(solution)/shard_map/dot_general | solution.py:49
  70.4 8.3 %fusion.9 = bf16[3072,256]{0,1:T(8,128)(2,1)} fusion(bf16[1,768,3072]{2,1,0:T(8,128)(2,1)} %param.16, bf16[256,3072]{1,0:T(8,128)(2,1)S(1)} %copy-done.8, bf16[1,3072,768]{2,1,0:T(8,128)(2,1)} %param.15, f32[256,768]{1,0:T(8,128)S(1)} %fusion.4), kind=kOutput, calls=%fused_computation.11 | convolution fusion | flops 2417885184 | bytes 13369344 | tf_op jit(solution)/shard_map/dot_general | solution.py:55
  78.7 0.7 fusion.43
  79.7 27.2 %reduce-scatter.2.cloned.1.call-done = bf16[768,256]{0,1:T(8,128)(2,1)} async-done(((bf16[3072,256]{0,1:T(8,128)(2,1)}), bf16[768,256]{0,1:T(8,128)(2,1)}) %reduce-scatter.2.cloned.1.call-update) | async-done | bytes 393232 | tf_op jit(solution)/shard_map/reduce_scatter | solution.py:54
  106.9 1.1 multiply_convert_fusion.1
  108.1 2.2 %gather_fusion.2 = bf16[384,768]{1,0:T(8,128)(2,1)S(1)} fusion(bf16[768,256]{0,1:T(8,128)(2,1)S(1)} %multiply_convert_fusion.1, s32[1024]{0:T(1024)S(1)} %pad_clamp_fusion), kind=kCustom, calls=%fused_computation.2 | custom fusion | bytes 1181184 | tf_op jit(solution)/shard_map/jit(_take)/gather | solution.py:64
  110.3 0.9 broadcast_select_fusion.1
  111.2 5.5 %all-to-all-start.1 = ((bf16[768,8,48]{0,2,1:T(8,128)(2,1)}), bf16[768,8,48]{0,2,1:T(8,128)(2,1)S(1)}, u32[]{:S(2)}, u32[]{:S(2)}) async-start(bf16[768,8,48]{0,2,1:T(8,128)(2,1)} %broadcast_select_fusion.1), calls=%async_computation.2 | async-start | bytes 1179648 | tf_op jit(solution)/shard_map/all_to_all | solution.py:65
  117.0 15.5 %all-to-all-done.1 = bf16[768,8,48]{0,2,1:T(8,128)(2,1)S(1)} async-done(((bf16[768,8,48]{0,2,1:T(8,128)(2,1)}), bf16[768,8,48]{0,2,1:T(8,128)(2,1)S(1)}, u32[]{:S(2)}, u32[]{:S(2)}) %all-to-all-start.1) | async-done | bytes 589856 | tf_op jit(solution)/shard_map/all_to_all | solution.py:65
  132.5 1.8 %multiply_reduce_fusion.1 = (f32[256]{0:T(256)S(1)}, f32[256,768]{1,0:T(8,128)S(1)}) fusion(bf16[768,384]{0,1:T(8,128)(2,1)S(1)} %bitcast.73, s32[384]{0:T(512)S(1)} %subtract_select_fusion, pred[384]{0:T(512)(128)(4,1)S(1)} %lt.182, f32[256,3072]{1,0:T(8,128)} %copy-done.1, s32[]{:T(128)S(6)} %select_n.231), kind=kOutput, calls=%fused_computation.17 | convolution fusion | flops 151781120 | bytes 2165636 | tf_op jit(solution)/shard_map/dot_general | solution.py:70
  134.3 5.9 %psum.7 = f32[256]{0:T(256)S(1)} all-reduce(f32[256]{0:T(256)S(1)} %get-tuple-element.53), channel_id=1, replica_groups=mesh['ep'=8,'tp'=4] {'tp'}, use_global_device_ids=true, to_apply=%region_5.7 | all-reduce | flops 256 | bytes 2048 | tf_op jit(solution)/shard_map/psum | solution.py:78
  140.2 0.9 multiply_convert_fusion
  (50 shorter events, 1.8 us)
Async XLA Ops:
  6.5 4.3 %copy-start = (s32[8,256]{1,0:T(8,128)S(1)}, s32[8,256]{1,0:T(8,128)}, u32[]{:S(2)}) copy-start(s32[8,256]{1,0:T(8,128)} %param.12) | copy-start | bytes 24580
  10.1 9.8 %copy-start.1 = (f32[256,3072]{1,0:T(8,128)}, f32[256,3072]{1,0:T(8,128)S(1)}, u32[]{:S(2)}) copy-start(f32[256,3072]{1,0:T(8,128)S(1)} %convert_element_type.34) | copy-start | bytes 9437188
  10.1 6.2 %copy-start.5 = (bf16[3072]{0:T(1024)(128)(2,1)S(1)}, bf16[3072]{0:T(1024)(128)(2,1)}, u32[]{:S(2)}) copy-start(bf16[3072]{0:T(1024)(128)(2,1)} %param.11) | copy-start | bytes 18436
  11.2 0.6 copy-start.2
  15.6 0.7 copy-start.3
  21.9 23.2 %all-to-all-start = ((bf16[8,48,768]{2,1,0:T(8,128)(2,1)}), bf16[8,48,768]{2,1,0:T(8,128)(2,1)S(1)}, u32[]{:S(2)}, u32[]{:S(2)}) async-start(bf16[8,48,768]{2,1,0:T(8,128)(2,1)} %broadcast_select_fusion), calls=%async_computation | async-start | bytes 1179648 | tf_op jit(solution)/shard_map/all_to_all | solution.py:46
  29.2 36.8 %all-gather.2.cloned.1.call-start = ((), (), s32[]{:S(2)}) async-start(), calls=%async_computation.3 | async-start | bytes 1966080 | tf_op jit(solution)/shard_map/all_gather | solution.py:48
  47.1 59.8 %reduce-scatter.2.cloned.1.call-start = ((), (), s32[]{:S(2)}) async-start(), calls=%async_computation.4 | async-start | bytes 1966080 | tf_op jit(solution)/shard_map/reduce_scatter | solution.py:54
  66.0 4.3 %copy-start.8 = (bf16[256,3072]{1,0:T(8,128)(2,1)S(1)}, bf16[256,3072]{1,0:T(8,128)(2,1)}, u32[]{:S(2)}) copy-start(bf16[256,3072]{1,0:T(8,128)(2,1)} %all-gather.2.cloned.1.call-done) | copy-start | bytes 4718596
  70.3 36.6 %copy-start.7 = (f32[1,256]{1,0:T(1,128)S(1)}, f32[1,256]{1,0:T(1,128)}, u32[]{:S(2)}) copy-start(f32[1,256]{1,0:T(1,128)} %param.13) | copy-start | bytes 3076
  108.1 8.7 %copy-start.4 = (pred[8,48]{1,0:T(8,128)(4,1)S(1)}, pred[8,48]{1,0:T(8,128)(4,1)}, u32[]{:S(2)}) copy-start(pred[8,48]{1,0:T(8,128)(4,1)} %copy-done.3) | copy-start | bytes 1156
  108.1 8.8 %copy-start.6 = (bf16[768]{0:T(1024)(128)(2,1)S(1)}, bf16[768]{0:T(1024)(128)(2,1)}, u32[]{:S(2)}) copy-start(bf16[768]{0:T(1024)(128)(2,1)} %param.17) | copy-start | bytes 4612
  111.2 21.3 %all-to-all-start.1 = ((bf16[768,8,48]{0,2,1:T(8,128)(2,1)}), bf16[768,8,48]{0,2,1:T(8,128)(2,1)S(1)}, u32[]{:S(2)}, u32[]{:S(2)}) async-start(bf16[768,8,48]{0,2,1:T(8,128)(2,1)} %broadcast_select_fusion.1), calls=%async_computation.2 | async-start | bytes 1179648 | tf_op jit(solution)/shard_map/all_to_all | solution.py:65
Sparse Core Ops, SparseCore 0:
  47.3 18.7 all-gather.1
  78.8 28.0 reduce-scatter.1
where the time goes:
time: 149 us; the launch traced here: 148 us
  waiting for transfers between devices  70.9 us (48%)
  other arithmetic  19.3 us (13%)
  matrix products  14.5 us (10%)
  between operations  13.6 us (9%)
  starting transfers between devices  12.9 us (9%)
  local copies, waits for them, and re-layouts  10.8 us (7%)
  blocking collectives  5.92 us (4%)
    reduce_scatter x1, waiting for transfers between devices, on_device(): lax.psum_scatter(lax.dot_general(piece, hidden, (((0,), (1,)), ((), ())),...  27.2 us
    all_gather x1, waiting for transfers between devices, on_device(): piece = lax.all_gather(shared, 'tp', axis=1, tiled=True)  18.8 us
    all_to_all x1, waiting for transfers between devices, on_device(): lax.all_to_all(leaving, 'ep', split_axis=1, concat_axis=1, tiled=True)  15.5 us
    all_to_all x1, waiting for transfers between devices, on_device(): lax.all_to_all(outgoing, 'ep', split_axis=0, concat_axis=0, tiled=True)  9.39 us
    dot_general x1, matrix products, on_device(): lax.dot_general(piece, hidden, (((0,), (1,)), ((), ())), preferred_elemen...  8.34 us
    all_to_all x1, starting transfers between devices, on_device(): lax.all_to_all(outgoing, 'ep', split_axis=0, concat_axis=0, tiled=True)  7.28 us
    psum x1, blocking collectives, on_device(): totals = lax.psum(jnp.sum(merged * merged, axis=1), 'tp')  5.92 us
    all_to_all x1, starting transfers between devices, on_device(): lax.all_to_all(leaving, 'ep', split_axis=1, concat_axis=1, tiled=True)  5.51 us
  transfers between devices with their start and end apart: 4, of which 4 were waited for; matrix products, arithmetic and copies ran while one was open for 5% of the time, Pallas kernels for 0%

commit v1 on v0

v1 whole, which is shorter than its diff:
```python
import functools

import jax
import jax.numpy as jnp
from jax import lax
from jax.experimental import pallas as pl
from jax.experimental.pallas import tpu as pltpu
from jax.sharding import PartitionSpec as P

EPSILON = 1e-06
F32 = jnp.float32
BF16 = jnp.bfloat16
MESH = pl.DeviceIdType.MESH


def layer(
    experts, tp, chunks, slots,
    stream_hbm, gain_ref, chosen_ref, aff_ref, wg_hbm, wu_hbm, wd_hbm, fgain_ref,
    out_ref,
    x_v, xn_v, wg_v, wu_v, wd_v, sel_v, place_v, pack_v, spread_v, aff_v,
    send_v, recv_v, piece_v, accg_v, accu_v, hidden_v,
    psend_v, pown_v, prec_v, ysend_v, yrec_v, leave_v, ret_v, merged_v, ssq_v,
    x_sem, w_sem, wd_sem,
    dsend, drecv, gsend, grecv, fsend, frecv, psend, precv, ysend, yrecv,
    rsend, rrecv, qsend, qrecv,
):
    me = lax.axis_index("ep")
    col = lax.axis_index("tp")
    tok = x_v.shape[0]
    width = x_v.shape[1]
    share = xn_v.shape[1]
    caps = chosen_ref.shape[1]
    cw = share // chunks
    rows = experts * slots
    chips = tp // 2
    y = col // 2
    core = col % 2
    partner = y * 2 + 1 - core

    barrier = pltpu.get_barrier_semaphore()
    for r in range(1, experts):
        pl.semaphore_signal(barrier, inc=1, device_id={"ep": (me + r) % experts}, device_id_type=MESH)
    for r in range(1, tp):
        pl.semaphore_signal(barrier, inc=1, device_id={"tp": (col + r) % tp}, device_id_type=MESH)

    x_copy = pltpu.make_async_copy(stream_hbm, x_v, x_sem)
    x_copy.start()
    w_copies = []
    for k in range(chunks):
        group = []
        for n, (src, dst) in enumerate(((wg_hbm, wg_v), (wu_hbm, wu_v))):
            for j in range(tp):
                copy = pltpu.make_async_copy(
                    src.at[pl.ds(j * share + k * cw, cw), :],
                    dst.at[k, pl.ds(j * cw, cw), :],
                    w_sem.at[k, n, j],
                )
                copy.start()
                group.append(copy)
        w_copies.append(group)
    wd_copy = pltpu.make_async_copy(wd_hbm, wd_v, wd_sem)
    wd_copy.start()

    base = (me * tok).astype(F32)
    lane_cap = lax.broadcasted_iota(jnp.int32, (slots, caps), 1).astype(F32)
    sub_slot = lax.broadcasted_iota(jnp.int32, (slots, caps), 0).astype(F32)
    lane_tok = lax.broadcasted_iota(jnp.int32, (slots, tok), 1).astype(F32)

    def build_sel(e, carry):
        row = chosen_ref[pl.ds(e, 1), :].astype(F32)
        start = jnp.sum(jnp.where(row < base, 1.0, 0.0), axis=1, keepdims=True)
        hit = lane_cap == sub_slot + start
        token = jnp.sum(jnp.where(hit, row + 1.0, 0.0), axis=1, keepdims=True) - 1.0 - base
        sel_v[e] = jnp.where(token == lane_tok, 1.0, 0.0).astype(BF16)
        return carry

    lax.fori_loop(0, experts, build_sel, 0)

    x_copy.wait()
    gain = gain_ref[:, pl.ds(pl.multiple_of(col * share, 128), share)]
    step_rows = 16

    def norm_rows(i, carry):
        at = pl.ds(pl.multiple_of(i * step_rows, step_rows), step_rows)
        block = x_v[at, :].astype(F32)
        scale = lax.rsqrt(jnp.sum(block * block, axis=1, keepdims=True) / width + EPSILON)
        own = x_v[at, pl.ds(pl.multiple_of(col * share, 128), share)].astype(F32)
        xn_v[at, :] = (own * scale * gain).astype(BF16)
        return carry

    lax.fori_loop(0, tok // step_rows, norm_rows, 0)

    pl.semaphore_wait(barrier, experts - 1 + tp - 1)

    sel = sel_v[...].reshape(rows, tok)
    finish = []

    def exchange(k, src, dst, ssem, rsem):
        for r in range(1, experts):
            to = (me + r) % experts
            copy = pltpu.make_async_remote_copy(
                src_ref=src.at[k, to], dst_ref=dst.at[k, me],
                send_sem=ssem.at[k, r], recv_sem=rsem.at[k, r],
                device_id={"ep": to}, device_id_type=MESH,
            )
            copy.start()
            finish.append(copy)
        dst[k, me] = src[k, me]

    def exchange_wait(k, src, dst, ssem, rsem):
        for r in range(1, experts):
            frm = (me + experts - r) % experts
            pltpu.make_async_remote_copy(
                src_ref=src.at[k, me], dst_ref=dst.at[k, frm],
                send_sem=ssem.at[k, r], recv_sem=rsem.at[k, r],
                device_id={"ep": frm}, device_id_type=MESH,
            ).wait_recv()

    for k in range(chunks):
        out = jnp.dot(sel, xn_v[:, k * cw:(k + 1) * cw], preferred_element_type=F32)
        send_v[k] = out.astype(BF16).reshape(experts, slots, cw)
        exchange(k, send_v, recv_v, dsend, drecv)

    own_row = chosen_ref[pl.ds(me, 1), :].astype(F32)
    lane_j = lax.broadcasted_iota(jnp.int32, (1, rows), 1).astype(F32)
    start_j = jnp.zeros((1, rows), F32)
    end_j = jnp.zeros((1, rows), F32)
    slot_j = lane_j
    start_d = jnp.zeros((1, 1), F32)
    for d in range(experts):
        end_d = jnp.sum(jnp.where(own_row < float((d + 1) * tok), 1.0, 0.0), axis=1, keepdims=True)
        mine = (lane_j >= float(d * slots)) & (lane_j < float((d + 1) * slots))
        start_j = start_j + jnp.where(mine, start_d, 0.0)
        end_j = end_j + jnp.where(mine, end_d, 0.0)
        slot_j = slot_j - jnp.where(mine, float(d * slots), 0.0)
        spread_v[d] = jnp.where(
            (lane_cap == sub_slot + start_d) & (lane_cap < end_d), 1.0, 0.0
        ).astype(BF16)
        start_d = end_d
    want = start_j + slot_j
    part = 32

    def build_pack(i, carry):
        at = pl.multiple_of(i * part, part)
        pick = (lax.broadcasted_iota(jnp.int32, (part, rows), 0) + at).astype(F32)
        pack_v[pl.ds(at, part), :] = jnp.where((pick == want) & (pick < end_j), 1.0, 0.0).astype(BF16)
        return carry

    lax.fori_loop(0, caps // part, build_pack, 0)

    square = 128
    eye = (
        lax.broadcasted_iota(jnp.int32, (square, square), 0)
        == lax.broadcasted_iota(jnp.int32, (square, square), 1)
    )
    for b in range(caps // square):
        weights = aff_ref[:, b * square:(b + 1) * square]
        aff_v[b * square:(b + 1) * square, :] = jnp.sum(
            jnp.where(eye, weights, 0.0), axis=1, keepdims=True
        )
    for b in range(rows // square):
        block = sel.astype(F32)[b * square:(b + 1) * square, :]
        place_v[:, b * square:(b + 1) * square] = block.T.astype(BF16)

    def part_of(k, j):
        return piece_v.at[k, :, pl.ds(pl.multiple_of(j * cw, 128), cw)]

    def gather_start(k):
        exchange_wait(k, send_v, recv_v, dsend, drecv)
        got = recv_v[k].reshape(rows, cw)
        own = jnp.dot(pack_v[...], got, preferred_element_type=F32).astype(BF16)
        piece_v[k, :, pl.ds(pl.multiple_of(col * cw, 128), cw)] = own
        for r in range(1, chips):
            to = ((y + r) % chips) * 2 + core
            copy = pltpu.make_async_remote_copy(
                src_ref=part_of(k, col), dst_ref=part_of(k, col),
                send_sem=gsend.at[k, r], recv_sem=grecv.at[k, r],
                device_id={"tp": to}, device_id_type=MESH,
            )
            copy.start()
            finish.append(copy)
        copy = pltpu.make_async_remote_copy(
            src_ref=part_of(k, col), dst_ref=part_of(k, col),
            send_sem=fsend.at[k, 0], recv_sem=frecv.at[k, 0],
            device_id={"tp": partner}, device_id_type=MESH,
        )
        copy.start()
        finish.append(copy)

    def gather_finish(k):
        for r in range(1, chips):
            frm = ((y + chips - r) % chips) * 2 + core
            pltpu.make_async_remote_copy(
                src_ref=part_of(k, col), dst_ref=part_of(k, frm),
                send_sem=gsend.at[k, r], recv_sem=grecv.at[k, r],
                device_id={"tp": frm}, device_id_type=MESH,
            ).wait_recv()
            copy = pltpu.make_async_remote_copy(
                src_ref=part_of(k, frm), dst_ref=part_of(k, frm),
                send_sem=fsend.at[k, r], recv_sem=frecv.at[k, r],
                device_id={"tp": partner}, device_id_type=MESH,
            )
            copy.start()
            finish.append(copy)
        for copy in w_copies[k]:
            copy.wait()
        for r in range(chips):
            theirs = ((y + chips - r) % chips) * 2 + 1 - core
            pltpu.make_async_remote_copy(
                src_ref=part_of(k, col), dst_ref=part_of(k, theirs),
                send_sem=fsend.at[k, r], recv_sem=frecv.at[k, r],
                device_id={"tp": partner}, device_id_type=MESH,
            ).wait_recv()
        taken = piece_v[k]
        gate = jnp.dot(taken, wg_v[k], preferred_element_type=F32)
        accg_v[...] = gate if k == 0 else accg_v[...] + gate
        up = jnp.dot(taken, wu_v[k], preferred_element_type=F32)
        accu_v[...] = up if k == 0 else accu_v[...] + up

    for k in range(chunks):
        gather_start(k)
        if k > 0:
            gather_finish(k - 1)
    gather_finish(chunks - 1)

    hblock = 32

    def activate(i, carry):
        at = pl.ds(pl.multiple_of(i * hblock, hblock), hblock)
        gate = accg_v[at, :]
        hidden_v[at, :] = (gate / (1.0 + jnp.exp(-gate)) * accu_v[at, :]).astype(BF16)
        return carry

    lax.fori_loop(0, caps // hblock, activate, 0)
    wd_copy.wait()

    def down(k, j):
        at = pl.ds(pl.multiple_of(j * share + k * cw, 128), cw)
        return jnp.dot(hidden_v[...], wd_v[:, at], preferred_element_type=F32)

    def pair_copy(k, r):
        return pltpu.make_async_remote_copy(
            src_ref=psend_v.at[k, r], dst_ref=prec_v.at[k, r],
            send_sem=psend.at[k, r], recv_sem=precv.at[k, r],
            device_id={"tp": partner}, device_id_type=MESH,
        )

    order = [r for r in range(1, chips)] + [0]

    def stage_pair(k):
        for r in order:
            to = (y + r) % chips
            psend_v[k, r] = down(k, to * 2 + 1 - core).astype(BF16)
            copy = pair_copy(k, r)
            copy.start()
            finish.append(copy)
        for r in order:
            to = (y + r) % chips
            pown_v[k, r] = down(k, to * 2 + core)

    def chip_copy(k, r):
        to = ((y + r) % chips) * 2 + core
        return pltpu.make_async_remote_copy(
            src_ref=ysend_v.at[k, r], dst_ref=yrec_v.at[k, r],
            send_sem=ysend.at[k, r], recv_sem=yrecv.at[k, r],
            device_id={"tp": to}, device_id_type=MESH,
        )

    def stage_chip(k):
        for r in order:
            pair_copy(k, r).wait_recv()
            both = pown_v[k, r] + prec_v[k, r].astype(F32)
            if r == 0:
                pown_v[k, r] = both
            else:
                ysend_v[k, r] = both.astype(BF16)
                copy = chip_copy(k, r)
                copy.start()
                finish.append(copy)

    def stage_leave(k):
        total = pown_v[k, 0]
        for r in range(1, chips):
            chip_copy(k, r).wait_recv()
            total = total + yrec_v[k, r].astype(F32)
        weighted = (total * aff_v[...]).astype(BF16)
        spread = spread_v[...].reshape(rows, caps)
        out = jnp.dot(spread, weighted, preferred_element_type=F32)
        leave_v[k] = out.astype(BF16).reshape(experts, slots, cw)
        exchange(k, leave_v, ret_v, rsend, rrecv)

    for k in range(chunks):
        stage_pair(k)
        if k > 0:
            stage_chip(k - 1)
    stage_chip(chunks - 1)
    for k in range(chunks):
        stage_leave(k)

    squares = jnp.zeros((tok, 1), F32)
    for k in range(chunks):
        exchange_wait(k, leave_v, ret_v, rsend, rrecv)
        update = jnp.dot(place_v[...], ret_v[k].reshape(rows, cw), preferred_element_type=F32)
        at = pl.ds(pl.multiple_of(col * share + k * cw, 128), cw)
        merged = x_v[:, at].astype(F32) + update
        merged_v[k] = merged
        squares = squares + jnp.sum(merged * merged, axis=1, keepdims=True)

    for b in range(tok // square):
        line = jnp.sum(
            jnp.where(eye, squares[b * square:(b + 1) * square, :], 0.0), axis=0, keepdims=True
        )
        ssq_v[0, :, b * square:(b + 1) * square] = jnp.broadcast_to(line, (8, square))

    def square_copy(r):
        return pltpu.make_async_remote_copy(
            src_ref=ssq_v.at[0], dst_ref=ssq_v.at[r],
            send_sem=qsend.at[r], recv_sem=qrecv.at[r],
            device_id={"tp": (col + r) % tp}, device_id_type=MESH,
        )

    for r in range(1, tp):
        copy = square_copy(r)
        copy.start()
        finish.append(copy)
    sums = ssq_v[0]
    for r in range(1, tp):
        square_copy(r).wait_recv()
        sums = sums + ssq_v[r]
    for b in range(tok // square):
        line = sums[0:1, b * square:(b + 1) * square]
        column = jnp.sum(jnp.where(eye, line, 0.0), axis=1, keepdims=True)
        scale = lax.rsqrt(column / width + EPSILON)
        for k in range(chunks):
            block = merged_v[k, b * square:(b + 1) * square, :]
            out_ref[b * square:(b + 1) * square, k * cw:(k + 1) * cw] = (
                block * scale * fgain_ref[:, k * cw:(k + 1) * cw]
            ).astype(BF16)

    for copy in finish:
        copy.wait_send()


def on_device(stream, ffn_gain, chosen, affinity, w_gate, w_up, w_down, final_gain):
    tok, width = stream.shape
    experts, caps = chosen.shape
    tp = lax.axis_size("tp")
    share = width // tp
    hid = w_gate.shape[2]
    slots = 3 * tok // 16
    chunks = 3 if share % 384 == 0 else 1
    cw = share // chunks
    chips = tp // 2
    rows = experts * slots
    vmem = pl.BlockSpec(memory_space=pltpu.VMEM)
    hbm = pl.BlockSpec(memory_space=pl.ANY)
    dma = pltpu.SemaphoreType.DMA
    return pl.pallas_call(
        functools.partial(layer, experts, tp, chunks, slots),
        out_shape=jax.ShapeDtypeStruct((tok, share), BF16),
        in_specs=[hbm, vmem, vmem, vmem, hbm, hbm, hbm, vmem],
        out_specs=vmem,
        scratch_shapes=[
            pltpu.VMEM((tok, width), BF16),
            pltpu.VMEM((tok, share), BF16),
            pltpu.VMEM((chunks, tp * cw, hid), BF16),
            pltpu.VMEM((chunks, tp * cw, hid), BF16),
            pltpu.VMEM((hid, width), BF16),
            pltpu.VMEM((experts, slots, tok), BF16),
            pltpu.VMEM((tok, rows), BF16),
            pltpu.VMEM((caps, rows), BF16),
            pltpu.VMEM((experts, slots, caps), BF16),
            pltpu.VMEM((caps, 1), F32),
            pltpu.VMEM((chunks, experts, slots, cw), BF16),
            pltpu.VMEM((chunks, experts, slots, cw), BF16),
            pltpu.VMEM((chunks, caps, tp * cw), BF16),
            pltpu.VMEM((caps, hid), F32),
            pltpu.VMEM((caps, hid), F32),
            pltpu.VMEM((caps, hid), BF16),
            pltpu.VMEM((chunks, chips, caps, cw), BF16),
            pltpu.VMEM((chunks, chips, caps, cw), F32),
            pltpu.VMEM((chunks, chips, caps, cw), BF16),
            pltpu.VMEM((chunks, chips, caps, cw), BF16),
            pltpu.VMEM((chunks, chips, caps, cw), BF16),
            pltpu.VMEM((chunks, experts, slots, cw), BF16),
            pltpu.VMEM((chunks, experts, slots, cw), BF16),
            pltpu.VMEM((chunks, tok, cw), F32),
            pltpu.VMEM((tp, 8, tok), F32),
            dma, dma((chunks, 2, tp)), dma,
            dma((chunks, experts)), dma((chunks, experts)),
            dma((chunks, chips)), dma((chunks, chips)),
            dma((chunks, chips)), dma((chunks, chips)),
            dma((chunks, chips)), dma((chunks, chips)),
            dma((chunks, chips)), dma((chunks, chips)),
            dma((chunks, experts)), dma((chunks, experts)),
            dma((tp,)), dma((tp,)),
        ],
        compiler_params=pltpu.CompilerParams(
            collective_id=0, has_side_effects=True, vmem_limit_bytes=60 * 1024 * 1024
        ),
        name="layer",
    )(
        stream,
        ffn_gain.astype(F32)[None, :],
        chosen,
        affinity,
        w_gate[0],
        w_up[0],
        w_down[0],
        final_gain.astype(F32)[None, :],
    )


def solution(mesh):
    return jax.shard_map(
        on_device,
        mesh=mesh,
        in_specs=(
            P("ep", None),
            P(),
            P(),
            P("ep", None),
            P("ep", None, "tp"),
            P("ep", None, "tp"),
            P("ep", "tp", None),
            P("tp"),
        ),
        out_specs=P("ep", "tp"),
        check_vma=False,
    )
```

time: 149 us -> 63.6 us (0.43)
  waiting for transfers between devices: 70.9 us -> 0 us
  Pallas kernels: 0 us -> 59 us
  other arithmetic: 19.3 us -> 1.29 us
  matrix products: 14.5 us -> 0 us
  between operations: 13.6 us -> 0.01 us
  starting transfers between devices: 12.9 us -> 0 us
  local copies, waits for them, and re-layouts: 10.8 us -> 3.03 us
  blocking collectives: 5.92 us -> 0 us
    pallas_call x0 -> x1, Pallas kernels: none -> 59 us  [on_device(): pl.pallas_call(functools.partial(layer, experts, tp, chunks, slots), out_...]
    reduce_scatter x1 -> x0, waiting for transfers between devices: 27.2 us -> none  [on_device(): lax.psum_scatter(lax.dot_general(piece, hidden, (((0,), (1,)), ((), ())),...]
    all_to_all x2 -> x0, waiting for transfers between devices: 24.8 us -> none  [the longest x1 15.5 us: on_device(): lax.all_to_all(leaving, 'ep', split_axis=1, concat_axis=1, tiled=True)]
    all_gather x1 -> x0, waiting for transfers between devices: 18.8 us -> none  [on_device(): piece = lax.all_gather(shared, 'tp', axis=1, tiled=True)]
    dot_general x3 -> x0, matrix products: 14.5 us -> none  [the longest x1 8.34 us: on_device(): lax.dot_general(piece, hidden, (((0,), (1,)), ((), ())), preferred_elemen...]
    all_to_all x2 -> x0, starting transfers between devices: 12.8 us -> none  [the longest x1 7.28 us: on_device(): lax.all_to_all(outgoing, 'ep', split_axis=0, concat_axis=0, tiled=True)]
    gather x7 -> x0, local copies, waits for them, and re-layouts: 9.71 us -> none  [the longest x3 2.9 us: on_device(): jnp.take_along_axis(chosen, send_pos, axis=1) - device * tok_rows]
    psum x1 -> x0, blocking collectives: 5.92 us -> none  [on_device(): totals = lax.psum(jnp.sum(merged * merged, axis=1), 'tp')]
  transfers between devices with their start and end apart: 4 -> 0, of which waited for: 4 -> 0; matrix products, arithmetic and copies ran while one was open for 5% -> 0% of each run, Pallas kernels for 0% -> 0%
where the time goes in v1:
time: 63.6 us; the launch traced here: 63.3 us
  Pallas kernels  59 us (93%)
  local copies, waits for them, and re-layouts  3.03 us (5%)
  other arithmetic  1.29 us (2%)
    pallas_call x1, Pallas kernels, on_device(): pl.pallas_call(functools.partial(layer, experts, tp, chunks, slots), out_...  59 us
    unnamed x1, local copies, waits for them, and re-layouts  1.77 us
    broadcast_in_dim x1, other arithmetic, on_device(): ffn_gain.astype(F32)[None, :]  1.29 us

profile of v1, /device:TPU:0, one launch (start us, length us, event | category | flops | bytes accessed | tf_op | source)
XLA Modules:
  0.0 63.3 jit_solution(3888374799053871541)
XLA Ops:
  0.0 1.3 %reshape.1.fgain_ref = f32[1,768]{1,0:T(1,128)} reshape(bf16[768]{0:T(1024)(128)(2,1)} %param.15) | data formatting | bytes 4608 | tf_op jit(solution)/shard_map/broadcast_in_dim | solution.py:410
  1.3 1.3 %broadcast_in_dim.14 = f32[3072]{0:T(1024)} convert(bf16[3072]{0:T(1024)(128)(2,1)} %param.9) | non-fusion elementwise | flops 3072 | bytes 18432 | tf_op jit(solution)/shard_map/broadcast_in_dim | solution.py:404
  2.6 59.0 %layer.1 = bf16[256,768]{1,0:T(8,128)(2,1)} custom-call(bf16[256,3072]{1,0:T(8,128)(2,1)} %stream_hbm.1, f32[1,3072]{1,0:T(1,128)} %bitcast.7, s32[8,256]{1,0:T(8,128)} %chosen_ref.1, f32[1,256]{1,0:T(1,128)} %aff_ref.1, bf16[3072,768]{1,0:T(8,128)(2,1)} %bitcast.4, bf16[3072,768]{1,0:T(8,128)(2,1)} %bitcast.5, bf16[768,3072]{1,0:T(8,128)(2,1)} %bitcast.6, ...), custom_call_target="tpu_custom_call" | custom-call | tf_op jit(solution)/shard_map/layer/pallas_call | solution.py:358
  61.5 1.8 %copy.10 = bf16[256,768]{1,0:T(8,128)(2,1)} copy(bf16[256,768]{1,0:T(8,128)(2,1)} %layer.1) | data formatting | bytes 786432

commit v2 on v1

--- a/solution.py
+++ b/solution.py
@@ -19,7 +19,7 @@
     out_ref,
     x_v, xn_v, wg_v, wu_v, wd_v, sel_v, place_v, pack_v, spread_v, aff_v,
     send_v, recv_v, piece_v, accg_v, accu_v, hidden_v,
-    psend_v, pown_v, prec_v, ysend_v, yrec_v, leave_v, ret_v, merged_v, ssq_v,
+    psend_v, pown_v, prec_v, ysend_v, yrec_v, leave_v, ret_v, merged_v, ssq_v, gain_v,
     x_sem, w_sem, wd_sem,
     dsend, drecv, gsend, grecv, fsend, frecv, psend, precv, ysend, yrecv,
     rsend, rrecv, qsend, qrecv,
@@ -77,7 +77,11 @@
     lax.fori_loop(0, experts, build_sel, 0)
 
     x_copy.wait()
-    gain = gain_ref[:, pl.ds(pl.multiple_of(col * share, 128), share)]
+    gain_v[...] = gain_ref[...].astype(F32)
+    lines = share // 128
+    gain = jnp.concatenate(
+        [gain_v[pl.ds(col * lines + i, 1), :] for i in range(lines)], axis=1
+    )
     step_rows = 16
 
     def norm_rows(i, carry):
@@ -89,8 +93,6 @@
         return carry
 
     lax.fori_loop(0, tok // step_rows, norm_rows, 0)
-
-    pl.semaphore_wait(barrier, experts - 1 + tp - 1)
 
     sel = sel_v[...].reshape(rows, tok)
     finish = []
@@ -119,6 +121,8 @@
     for k in range(chunks):
         out = jnp.dot(sel, xn_v[:, k * cw:(k + 1) * cw], preferred_element_type=F32)
         send_v[k] = out.astype(BF16).reshape(experts, slots, cw)
+    pl.semaphore_wait(barrier, experts - 1 + tp - 1)
+    for k in range(chunks):
         exchange(k, send_v, recv_v, dsend, drecv)
 
     own_row = chosen_ref[pl.ds(me, 1), :].astype(F32)
@@ -245,16 +249,16 @@
             device_id={"tp": partner}, device_id_type=MESH,
         )
 
-    order = [r for r in range(1, chips)] + [0]
-
-    def stage_pair(k):
-        for r in order:
+    away = list(range(1, chips))
+
+    def stage_pair(k, turns):
+        for r in turns:
             to = (y + r) % chips
             psend_v[k, r] = down(k, to * 2 + 1 - core).astype(BF16)
             copy = pair_copy(k, r)
             copy.start()
             finish.append(copy)
-        for r in order:
+        for r in turns:
             to = (y + r) % chips
             pown_v[k, r] = down(k, to * 2 + core)
 
@@ -266,8 +270,8 @@
             device_id={"tp": to}, device_id_type=MESH,
         )
 
-    def stage_chip(k):
-        for r in order:
+    def stage_chip(k, turns):
+        for r in turns:
             pair_copy(k, r).wait_recv()
             both = pown_v[k, r] + prec_v[k, r].astype(F32)
             if r == 0:
@@ -290,11 +294,15 @@
         exchange(k, leave_v, ret_v, rsend, rrecv)
 
     for k in range(chunks):
-        stage_pair(k)
+        stage_pair(k, away)
         if k > 0:
-            stage_chip(k - 1)
-    stage_chip(chunks - 1)
-    for k in range(chunks):
+            stage_chip(k - 1, away)
+    stage_pair(0, [0])
+    stage_chip(chunks - 1, away)
+    for k in range(1, chunks):
+        stage_pair(k, [0])
+    for k in range(chunks):
+        stage_chip(k, [0])
         stage_leave(k)
 
     squares = jnp.zeros((tok, 1), F32)
@@ -303,7 +311,7 @@
         update = jnp.dot(place_v[...], ret_v[k].reshape(rows, cw), preferred_element_type=F32)
         at = pl.ds(pl.multiple_of(col * share + k * cw, 128), cw)
         merged = x_v[:, at].astype(F32) + update
-        merged_v[k] = merged
+        merged_v[:, k * cw:(k + 1) * cw] = merged
         squares = squares + jnp.sum(merged * merged, axis=1, keepdims=True)
 
     for b in range(tok // square):
@@ -323,6 +331,8 @@
         copy = square_copy(r)
         copy.start()
         finish.append(copy)
+    closing = fgain_ref[...].astype(F32)
+    fgain = jnp.concatenate([closing[i:i + 1, :] for i in range(lines)], axis=1)
     sums = ssq_v[0]
     for r in range(1, tp):
         square_copy(r).wait_recv()
@@ -331,11 +341,8 @@
         line = sums[0:1, b * square:(b + 1) * square]
         column = jnp.sum(jnp.where(eye, line, 0.0), axis=1, keepdims=True)
         scale = lax.rsqrt(column / width + EPSILON)
-        for k in range(chunks):
-            block = merged_v[k, b * square:(b + 1) * square, :]
-            out_ref[b * square:(b + 1) * square, k * cw:(k + 1) * cw] = (
-                block * scale * fgain_ref[:, k * cw:(k + 1) * cw]
-            ).astype(BF16)
+        at = slice(b * square, (b + 1) * square)
+        out_ref[at, :] = (merged_v[at, :] * scale * fgain).astype(BF16)
 
     for copy in finish:
         copy.wait_send()
@@ -353,39 +360,42 @@
     chips = tp // 2
     rows = experts * slots
     vmem = pl.BlockSpec(memory_space=pltpu.VMEM)
-    hbm = pl.BlockSpec(memory_space=pl.ANY)
+    hbm = pl.BlockSpec(memory_space=pltpu.HBM)
     dma = pltpu.SemaphoreType.DMA
+    buffers = [
+        pltpu.VMEM((tok, width), BF16),
+        pltpu.VMEM((tok, share), BF16),
+        pltpu.VMEM((chunks, tp * cw, hid), BF16),
+        pltpu.VMEM((chunks, tp * cw, hid), BF16),
+        pltpu.VMEM((hid, width), BF16),
+        pltpu.VMEM((experts, slots, tok), BF16),
+        pltpu.VMEM((tok, rows), BF16),
+        pltpu.VMEM((caps, rows), BF16),
+        pltpu.VMEM((experts, slots, caps), BF16),
+        pltpu.VMEM((caps, 1), F32),
+        pltpu.VMEM((chunks, experts, slots, cw), BF16),
+        pltpu.VMEM((chunks, experts, slots, cw), BF16),
+        pltpu.VMEM((chunks, caps, tp * cw), BF16),
+        pltpu.VMEM((caps, hid), F32),
+        pltpu.VMEM((caps, hid), F32),
+        pltpu.VMEM((caps, hid), BF16),
+        pltpu.VMEM((chunks, chips, caps, cw), BF16),
+        pltpu.VMEM((chunks, chips, caps, cw), F32),
+        pltpu.VMEM((chunks, chips, caps, cw), BF16),
+        pltpu.VMEM((chunks, chips, caps, cw), BF16),
+        pltpu.VMEM((chunks, chips, caps, cw), BF16),
+        pltpu.VMEM((chunks, experts, slots, cw), BF16),
+        pltpu.VMEM((chunks, experts, slots, cw), BF16),
+        pltpu.VMEM((tok, share), F32),
+        pltpu.VMEM((tp, 8, tok), F32),
+        pltpu.VMEM((width // 128, 128), F32),
+    ]
     return pl.pallas_call(
         functools.partial(layer, experts, tp, chunks, slots),
         out_shape=jax.ShapeDtypeStruct((tok, share), BF16),
         in_specs=[hbm, vmem, vmem, vmem, hbm, hbm, hbm, vmem],
         out_specs=vmem,
-        scratch_shapes=[
-            pltpu.VMEM((tok, width), BF16),
-            pltpu.VMEM((tok, share), BF16),
-            pltpu.VMEM((chunks, tp * cw, hid), BF16),
-            pltpu.VMEM((chunks, tp * cw, hid), BF16),
-            pltpu.VMEM((hid, width), BF16),
-            pltpu.VMEM((experts, slots, tok), BF16),
-            pltpu.VMEM((tok, rows), BF16),
-            pltpu.VMEM((caps, rows), BF16),
-            pltpu.VMEM((experts, slots, caps), BF16),
-            pltpu.VMEM((caps, 1), F32),
-            pltpu.VMEM((chunks, experts, slots, cw), BF16),
-            pltpu.VMEM((chunks, experts, slots, cw), BF16),
-            pltpu.VMEM((chunks, caps, tp * cw), BF16),
-            pltpu.VMEM((caps, hid), F32),
-            pltpu.VMEM((caps, hid), F32),
-            pltpu.VMEM((caps, hid), BF16),
-            pltpu.VMEM((chunks, chips, caps, cw), BF16),
-            pltpu.VMEM((chunks, chips, caps, cw), F32),
-            pltpu.VMEM((chunks, chips, caps, cw), BF16),
-            pltpu.VMEM((chunks, chips, caps, cw), BF16),
-            pltpu.VMEM((chunks, chips, caps, cw), BF16),
-            pltpu.VMEM((chunks, experts, slots, cw), BF16),
-            pltpu.VMEM((chunks, experts, slots, cw), BF16),
-            pltpu.VMEM((chunks, tok, cw), F32),
-            pltpu.VMEM((tp, 8, tok), F32),
+        scratch_shapes=buffers + [
             dma, dma((chunks, 2, tp)), dma,
             dma((chunks, experts)), dma((chunks, experts)),
             dma((chunks, chips)), dma((chunks, chips)),
@@ -401,13 +411,13 @@
         name="layer",
     )(
         stream,
-        ffn_gain.astype(F32)[None, :],
+        ffn_gain.reshape(width // 128, 128),
         chosen,
         affinity,
         w_gate[0],
         w_up[0],
         w_down[0],
-        final_gain.astype(F32)[None, :],
+        final_gain.reshape(share // 128, 128),
     )
 
 

time: 63.6 us -> 60.5 us (0.951)
  other arithmetic: 1.29 us -> 0 us
  local copies, waits for them, and re-layouts: 3.03 us -> 1.77 us
    broadcast_in_dim x1 -> x0, other arithmetic: 1.29 us -> none  [on_device(): ffn_gain.astype(F32)[None, :]]
    broadcast_in_dim x1 -> x0, local copies, waits for them, and re-layouts: 1.26 us -> none  [on_device(): final_gain.astype(F32)[None, :]]
where the time goes in v2:
time: 60.5 us; the launch traced here: 60.3 us
  Pallas kernels  58.5 us (97%)
  local copies, waits for them, and re-layouts  1.77 us (3%)
    pallas_call x1, Pallas kernels, on_device(): pl.pallas_call(functools.partial(layer, experts, tp, chunks, slots), out_...  58.5 us
    unnamed x1, local copies, waits for them, and re-layouts  1.77 us

profile of v2, /device:TPU:0, one launch (start us, length us, event | category | flops | bytes accessed | tf_op | source)
XLA Modules:
  0.0 60.3 jit_solution(12747121747299165515)
XLA Ops:
  0.0 58.5 %layer.1 = bf16[256,768]{1,0:T(8,128)(2,1)} custom-call(bf16[256,3072]{1,0:T(8,128)(2,1)} %stream_hbm.1, bf16[24,128]{1,0:T(8,128)(2,1)} %bitcast.8, s32[8,256]{1,0:T(8,128)} %chosen_ref.1, f32[1,256]{1,0:T(1,128)} %aff_ref.1, bf16[3072,768]{1,0:T(8,128)(2,1)} %bitcast.5, bf16[3072,768]{1,0:T(8,128)(2,1)} %bitcast.6, bf16[768,3072]{1,0:T(8,128)(2,1)} %bitcast.7, ...), custom_call_target="tpu_custom_call" | custom-call | tf_op jit(solution)/shard_map/layer/pallas_call | solution.py:393
  58.5 1.8 %copy.10 = bf16[256,768]{1,0:T(8,128)(2,1)} copy(bf16[256,768]{1,0:T(8,128)(2,1)} %layer.1) | data formatting | bytes 786432
